TPU v7x, 32 devices: a whole 2x2x4 slice. The times are simulated.
32 devices in a mesh: ep: 8 (over z, x), tp: 4 (over y, core).
Axes of the slice: x: 2, y: 2, z: 4, core: 2. Of those that a mesh axis runs over, the one named last changes fastest.
Arguments:
- tokens: bfloat16 [1024, 2048], P('ep'), may hold values from -6 to 6
- cotangent: bfloat16 [1024, 2048], P('ep'), may hold values from -1.5 to 1.5
- routes: int32 [1024, 2], P('ep'), may hold values from 0 to 3, all different within a row; in each aligned block of 128 rows (0 to 127, 128 to 255, ...) at most 96 rows name the same one
- router: bfloat16 [2048, 4], replicated, may hold values from -0.125 to 0.125
- w_gate: bfloat16 [8, 2048, 2048], P('ep', None, 'tp'), may hold values from -0.125 to 0.125
- w_up: bfloat16 [8, 2048, 2048], P('ep', None, 'tp'), may hold values from -0.125 to 0.125
- w_down: bfloat16 [8, 2048, 2048], P('ep', 'tp'), may hold values from -0.09375 to 0.09375
Outputs:
- token_grad: bfloat16 [1024, 2048], P('ep', 'tp')
- gate_grad: float32 [1024, 2], P('ep')
- grad_gate: bfloat16 [8, 2048, 2048], P('ep', None, 'tp')
- grad_up: bfloat16 [8, 2048, 2048], P('ep', None, 'tp')
- grad_down: bfloat16 [8, 2048, 2048], P('ep', 'tp')
- router_grad: float32 [2048, 4], P(('ep', 'tp'))
Inputs may be any that keep to these rules, and one draw needn't show every extreme that they name: `routes`: each row names 2 different experts. In the rows of one index of ep (aligned blocks of 128 rows) no expert is named by more than 96 rows, a bound that some block reaches.
All inputs are finite; a program needn't handle non-finite values.
Results may differ from a plain program's by a relative error of at most 0.018.
Values may be sent and summed in bfloat16 or wider, within the bound.
No kernel may reach another device: no remote copies, remote signals or barrier semaphores. Data moves between devices by JAX's collectives and lax.ppermute only.
A program may use at most 64 MiB of HBM per device.

v0:
```python
import jax
import jax.numpy as jnp
from jax import lax
from jax.sharding import PartitionSpec as P

BLOCKS = 2


def build_slots(block_routes, experts, capacity):
    flat_routes = block_routes.reshape(-1)
    labels = jnp.arange(experts, dtype=jnp.int32)
    hit_mask = (flat_routes[None, :] == labels[:, None]).astype(jnp.int32)
    rank_in = jnp.cumsum(hit_mask, axis=1, dtype=jnp.int32) - 1
    slot_ids = jnp.arange(capacity, dtype=jnp.int32)
    assigned = (hit_mask[:, None, :] == 1) & (rank_in[:, None, :] == slot_ids[None, :, None])
    return assigned.astype(jnp.float32)


def gate_pair(tokens, routes, router, experts):
    logits = jnp.dot(tokens, router, preferred_element_type=jnp.float32)
    labels = jnp.arange(experts, dtype=jnp.int32)
    picked = (routes[:, :, None] == labels[None, None, :]).astype(jnp.float32)
    chosen = jnp.sum(picked * logits[:, None, :], axis=2)
    margin = chosen[:, 0] - chosen[:, 1]
    weights = jnp.stack([jax.nn.sigmoid(margin), jax.nn.sigmoid(-margin)], axis=1)
    return (picked, weights)


def logit_grads(picked, weights, gate_grad):
    lead_grad = weights[:, 0] * weights[:, 1] * (gate_grad[:, 0] - gate_grad[:, 1])
    pair_grad = jnp.stack([lead_grad, -lead_grad], axis=1)
    return jnp.sum(picked * pair_grad[:, :, None], axis=1)


def expert_grads(rows_in, cot_in, gate_in, gate_weight, up_weight, down_weight):
    pre_gate = jnp.dot(rows_in, gate_weight, preferred_element_type=jnp.float32)
    pre_up = jnp.dot(rows_in, up_weight, preferred_element_type=jnp.float32)
    back_grad = lax.dot_general(
        cot_in, down_weight, (((1,), (1,)), ((), ())), preferred_element_type=jnp.float32
    )
    sig_gate = jax.nn.sigmoid(pre_gate)
    active = pre_gate * sig_gate
    hidden = (active * pre_up).astype(jnp.bfloat16)
    gate_terms = jnp.sum(hidden.astype(jnp.float32) * back_grad, axis=1)
    gate_col = gate_in.astype(jnp.float32)[:, None]
    scaled_back = gate_col * back_grad
    d_gate = (scaled_back * pre_up * sig_gate * (1.0 + pre_gate * (1.0 - sig_gate))).astype(
        jnp.bfloat16
    )
    d_up = (scaled_back * active).astype(jnp.bfloat16)
    scaled_cot = (gate_col * cot_in.astype(jnp.float32)).astype(jnp.bfloat16)
    contract_rows = (((0,), (0,)), ((), ()))
    grad_gate = lax.dot_general(
        rows_in, d_gate, contract_rows, preferred_element_type=jnp.float32
    ).astype(jnp.bfloat16)
    grad_up = lax.dot_general(
        rows_in, d_up, contract_rows, preferred_element_type=jnp.float32
    ).astype(jnp.bfloat16)
    grad_down = lax.dot_general(
        hidden, scaled_cot, contract_rows, preferred_element_type=jnp.float32
    ).astype(jnp.bfloat16)
    return (d_gate, d_up, gate_terms, grad_gate, grad_up, grad_down)


def spread_slabs(packed, experts, slab_count):
    widened = jnp.broadcast_to(packed[:, None], (experts, BLOCKS) + packed.shape[1:])
    return widened.reshape((slab_count,) + packed.shape[1:])


def shards(tokens, cotangent, routes, router, w_gate, w_up, w_down):
    highest = lax.Precision.HIGHEST
    ep_count = lax.axis_size("ep")
    tp_count = lax.axis_size("tp")
    experts = ep_count // BLOCKS
    tok_rows, width = tokens.shape
    top_count = routes.shape[1]
    capacity = 3 * tok_rows * top_count // (2 * experts)
    col_width = width // tp_count
    tp_index = lax.axis_index("tp")
    picked, weights = gate_pair(tokens, routes, router, experts)
    assigned = build_slots(routes, experts, capacity)
    per_token = jnp.sum(assigned.reshape(experts, capacity, tok_rows, top_count), axis=3)
    token_map = per_token.astype(jnp.bfloat16)
    gate_send = weights.astype(jnp.bfloat16)
    gate_slots = jnp.einsum(
        "ecj,j->ec", assigned, gate_send.astype(jnp.float32).reshape(-1), precision=highest
    ).astype(jnp.bfloat16)
    gate_out = spread_slabs(gate_slots, experts, ep_count)

    def pack_rows(source):
        packed = jnp.einsum(
            "ect,td->ecd", token_map, source, preferred_element_type=jnp.float32
        ).astype(jnp.bfloat16)
        return spread_slabs(packed, experts, ep_count)

    tok_part = lax.dynamic_slice_in_dim(tokens, tp_index * col_width, col_width, 1)
    cot_part = lax.dynamic_slice_in_dim(cotangent, tp_index * col_width, col_width, 1)
    recv_part, recv_cot_part, recv_gate = (
        lax.all_to_all(pack_rows(tok_part), "ep", split_axis=0, concat_axis=0, tiled=True),
        lax.all_to_all(pack_rows(cot_part), "ep", split_axis=0, concat_axis=0, tiled=True),
        lax.all_to_all(gate_out, "ep", split_axis=0, concat_axis=0, tiled=True),
    )
    recv_rows, recv_cot = (
        lax.all_gather(recv_part, "tp", axis=2, tiled=True),
        lax.all_gather(recv_cot_part, "tp", axis=2, tiled=True),
    )
    rows_in = recv_rows.reshape(-1, width)
    cot_in = recv_cot.reshape(-1, width)
    gate_in = recv_gate.reshape(-1)
    d_gate, d_up, gate_terms, grad_gate, grad_up, grad_down = expert_grads(
        rows_in, cot_in, gate_in, w_gate[0], w_up[0], w_down[0]
    )
    contract_hidden = (((1,), (1,)), ((), ()))
    partial_dx = lax.dot_general(
        d_gate, w_gate[0], contract_hidden, preferred_element_type=jnp.float32
    )
    partial_dx = partial_dx + lax.dot_general(
        d_up, w_up[0], contract_hidden, preferred_element_type=jnp.float32
    )
    summed_dx = lax.psum_scatter(
        partial_dx.reshape(ep_count, capacity, width).astype(jnp.bfloat16),
        "tp",
        scatter_dimension=2,
        tiled=True,
    ).astype(jnp.float32)
    gate_sums = lax.psum(gate_terms.reshape(ep_count, capacity), "tp")
    back_dx, back_gate = (
        lax.all_to_all(
            summed_dx.astype(jnp.bfloat16), "ep", split_axis=0, concat_axis=0, tiled=True
        ).astype(summed_dx.dtype),
        lax.all_to_all(
            gate_sums.astype(jnp.bfloat16), "ep", split_axis=0, concat_axis=0, tiled=True
        ).astype(gate_sums.dtype),
    )
    slab_dx = jnp.sum(back_dx.reshape(experts, BLOCKS, capacity, col_width), axis=1)
    routed_dx = jnp.einsum("ect,ecd->td", per_token, slab_dx, precision=highest)
    slab_gate = jnp.sum(back_gate.reshape(experts, BLOCKS, capacity), axis=1)
    gate_grad = jnp.einsum("ecj,ec->j", assigned, slab_gate, precision=highest).reshape(
        tok_rows, top_count
    )
    logit_grad = logit_grads(picked, weights, gate_grad)
    router_cols = lax.dynamic_slice_in_dim(router, tp_index * col_width, col_width, 0).astype(
        jnp.float32
    )
    token_grad = (routed_dx + jnp.dot(logit_grad, router_cols.T, precision=highest)).astype(
        jnp.bfloat16
    )
    seg_rows = tok_rows // tp_count
    own_rows = lax.dynamic_slice_in_dim(tokens, tp_index * seg_rows, seg_rows, 0).astype(
        jnp.float32
    )
    own_logit = lax.dynamic_slice_in_dim(logit_grad, tp_index * seg_rows, seg_rows, 0)
    router_grad = lax.psum_scatter(
        jnp.dot(own_rows.T, own_logit, precision=highest),
        ("ep", "tp"),
        scatter_dimension=0,
        tiled=True,
    )
    return (token_grad, gate_grad, grad_gate[None], grad_up[None], grad_down[None], router_grad)


def solution(mesh):
    placed = (
        P("ep", None),
        P("ep", None),
        P("ep", None),
        P(),
        P("ep", None, "tp"),
        P("ep", None, "tp"),
        P("ep", "tp", None),
    )
    return jax.shard_map(
        shards,
        mesh=mesh,
        in_specs=placed,
        out_specs=(
            P("ep", "tp"),
            P("ep", None),
            P("ep", None, "tp"),
            P("ep", None, "tp"),
            P("ep", "tp", None),
            P(("ep", "tp"), None),
        ),
        check_vma=False,
    )
```

profile of v0, /device:TPU:0, one launch (start us, length us, event | category | flops | bytes accessed | tf_op | source)
XLA Modules:
  0.0 325.1 jit_solution(1084350082928045645)
XLA Ops:
  7.2 0.9 copy.70
  8.3 1.2 reduce-window.6
  9.8 0.7 fusion.37
  10.9 1.2 convolution_convert_fusion.2
  12.1 27.3 %all_to_all.33 = bf16[8,96,512]{2,1,0:T(8,128)(2,1)} all-to-all(bf16[8,96,512]{2,1,0:T(8,128)(2,1)S(1)} %bitcast.80), channel_id=1, replica_groups=mesh['ep'=8,'tp'=4] {'ep'}, dimensions={0} | all-to-all | bytes 1572864 | tf_op jit(solution)/shard_map/all_to_all | solution.py:99
  39.5 1.2 convolution_convert_fusion.3
  40.8 23.3 %all_to_all.34 = bf16[8,96,512]{2,1,0:T(8,128)(2,1)} all-to-all(bf16[8,96,512]{2,1,0:T(8,128)(2,1)S(1)} %bitcast.81), channel_id=1, replica_groups=mesh['ep'=8,'tp'=4] {'ep'}, dimensions={0} | all-to-all | bytes 1572864 | tf_op jit(solution)/shard_map/all_to_all | solution.py:100
  64.5 0.2 fusion.45
  64.7 2.4 all-gather.5.cloned.1.call-done
  67.1 5.7 %fusion.11 = f32[768,512]{0,1:T(8,128)} fusion(bf16[768,2048]{1,0:T(8,128)(2,1)} %bitcast.95, bf16[1,2048,512]{2,1,0:T(8,128)(2,1)} %param.12), kind=kOutput, calls=%fused_computation.15 | convolution fusion | flops 1610612736 | bytes 6815744 | tf_op jit(solution)/shard_map/dot_general | solution.py:37
  72.8 3.0 fusion.8
  75.8 21.4 %all-gather.3.cloned.1.call-done = bf16[8,96,2048]{2,1,0:T(8,128)(2,1)} async-done(((bf16[8,96,512]{2,1,0:T(8,128)(2,1)}), bf16[8,96,2048]{2,1,0:T(8,128)(2,1)}) %all-gather.3.cloned.1.call-update) | async-done | bytes 3145744 | tf_op jit(solution)/shard_map/all_gather | solution.py:105
  97.2 6.7 %multiply_reduce_fusion = (f32[768]{0:T(1024)S(1)}, bf16[768,512]{0,1:T(8,128)(2,1)}, f32[768,512]{0,1:T(8,128)}) fusion(f32[768,512]{0,1:T(8,128)} %fusion.11, f32[768,512]{0,1:T(8,128)} %fusion.8, bf16[768,2048]{1,0:T(8,128)(2,1)} %bitcast.99, bf16[1,512,2048]{2,1,0:T(8,128)(2,1)} %param.13), kind=kOutput, calls=%fused_computation.20 | convolution fusion | flops 1614150912 | bytes 10750976 | tf_op jit(solution)/shard_map/dot_general | solution.py:38
  104.1 5.9 %psum.7 = bf16[8,96]{1,0:T(8,128)(2,1)S(1)} all-reduce(f32[8,96]{1,0:T(8,128)S(1)} %reshape.150), channel_id=1, replica_groups=mesh['ep'=8,'tp'=4] {'tp'}, use_global_device_ids=true, to_apply=%region_7.8 | all-reduce | flops 768 | bytes 4608 | tf_op jit(solution)/shard_map/psum | solution.py:126
  109.9 0.6 copy.80
  110.5 5.7 %all-to-all-start.4 = ((bf16[8,1,96]{2,1,0:T(2,128)(2,1)}), bf16[8,1,96]{2,1,0:T(2,128)(2,1)S(1)}, u32[]{:S(2)}, u32[]{:S(2)}) async-start(bf16[8,1,96]{2,1,0:T(2,128)(2,1)} %copy.80), calls=%async_computation.5 | async-start | bytes 8192 | tf_op jit(solution)/shard_map/all_to_all | solution.py:131
  116.5 6.1 %all-to-all-done.4 = bf16[8,1,96]{2,1,0:T(2,128)(2,1)S(1)} async-done(((bf16[8,1,96]{2,1,0:T(2,128)(2,1)}), bf16[8,1,96]{2,1,0:T(2,128)(2,1)S(1)}, u32[]{:S(2)}, u32[]{:S(2)}) %all-to-all-start.4) | async-done | bytes 1568 | tf_op jit(solution)/shard_map/all_to_all | solution.py:131
  123.4 8.9 %all_to_all.35 = bf16[8,1,96]{2,1,0:T(2,128)(2,1)S(1)} all-to-all(bf16[8,1,96]{2,1,0:T(2,128)(2,1)S(1)} %copy.77), channel_id=1, replica_groups=mesh['ep'=8,'tp'=4] {'ep'}, dimensions={0} | all-to-all | bytes 3072 | tf_op jit(solution)/shard_map/all_to_all | solution.py:101
  132.4 3.1 multiply_convert_fusion.7
  135.5 1.8 fusion.6
  137.4 0.3 copy-done.4
  137.7 3.5 %add_convert_fusion = bf16[768,2048]{1,0:T(8,128)(2,1)} fusion(f32[768,2048]{1,0:T(8,128)S(1)} %fusion.6, bf16[768,512]{0,1:T(8,128)(2,1)S(1)} %get-tuple-element.12, bf16[1,2048,512]{2,1,0:T(8,128)(2,1)S(1)} %copy-done.4), kind=kOutput, calls=%fused_computation.1 | convolution fusion | flops 1613758464 | bytes 12320768 | tf_op jit(solution)/shard_map/dot_general | solution.py:117
  141.4 1.8 fusion.31
  143.2 33.2 %reduce-scatter.5.cloned.1.call-done = bf16[8,96,512]{2,1,0:T(8,128)(2,1)} async-done(((bf16[8,96,2048]{2,1,0:T(8,128)(2,1)}), bf16[8,96,512]{2,1,0:T(8,128)(2,1)}) %reduce-scatter.5.cloned.1.call-update) | async-done | bytes 786448 | tf_op jit(solution)/shard_map/reduce_scatter | solution.py:120
  176.4 5.5 %all-to-all-start.3 = ((bf16[8,96,512]{2,1,0:T(8,128)(2,1)}), bf16[8,96,512]{2,1,0:T(8,128)(2,1)S(1)}, u32[]{:S(2)}, u32[]{:S(2)}) async-start(bf16[8,96,512]{2,1,0:T(8,128)(2,1)} %reduce-scatter.5.cloned.1.call-done), calls=%async_computation.4 | async-start | bytes 1572864 | tf_op jit(solution)/shard_map/all_to_all | solution.py:128
  181.9 5.4 %fusion.3 = bf16[1,2048,512]{2,1,0:T(8,128)(2,1)} fusion(bf16[768,2048]{1,0:T(8,128)(2,1)} %bitcast.96, bf16[768,512]{0,1:T(8,128)(2,1)} %copy-done.3), kind=kOutput, calls=%fused_computation.7 | convolution fusion | flops 1611661312 | bytes 6029312 | tf_op jit(solution)/shard_map/dot_general | solution.py:53
  187.3 3.2 fusion.5
  190.6 3.2 fusion.4
  193.8 121.5 %reduce-scatter.7.cloned.1.call-done = f32[64,4]{1,0:T(8,128)} async-done(((f32[2048,4]{1,0:T(8,128)}), f32[64,4]{1,0:T(8,128)}) %reduce-scatter.7.cloned.1.call-update) | async-done | bytes 1040
  315.3 1.4 copy.85
  316.9 0.7 convolution_bitcast_fusion
  317.6 1.0 fusion.16
  (73 shorter events, 2.8 us)
Async XLA Ops:
  7.2 65.6 %copy-start = (bf16[1,2048,512]{2,1,0:T(8,128)(2,1)S(1)}, bf16[1,2048,512]{2,1,0:T(8,128)(2,1)}, u32[]{:S(2)}) copy-start(bf16[1,2048,512]{2,1,0:T(8,128)(2,1)} %param.11) | copy-start | bytes 6291460
  7.2 60.0 %all-gather.5.cloned.1.call-start = ((), (), s32[]{:S(2)}) async-start(), calls=%async_computation.8 | async-start | bytes 3932160 | tf_op jit(solution)/shard_map/all_gather | solution.py:104
  39.4 24.9 %copy-start.7 = (s32[128,2]{0,1:T(2,128)S(1)}, s32[128,2]{0,1:T(2,128)}, u32[]{:S(2)}) copy-start(s32[128,2]{0,1:T(2,128)} %param.9) | copy-start | bytes 3076
  39.5 25.0 %copy-start.5 = (bf16[128,2048]{1,0:T(8,128)(2,1)S(1)}, bf16[128,2048]{1,0:T(8,128)(2,1)}, u32[]{:S(2)}) copy-start(bf16[128,2048]{1,0:T(8,128)(2,1)} %param.7) | copy-start | bytes 1572868
  39.5 25.0 %copy-start.6 = (bf16[2048,4]{0,1:T(4,128)(2,1)S(1)}, bf16[2048,4]{0,1:T(4,128)(2,1)}, u32[]{:S(2)}) copy-start(bf16[2048,4]{0,1:T(4,128)(2,1)} %param.10) | copy-start | bytes 49156
  39.5 57.8 %all-gather.3.cloned.1.call-start = ((), (), s32[]{:S(2)}) async-start(), calls=%async_computation.7 | async-start | bytes 3932160 | tf_op jit(solution)/shard_map/all_gather | solution.py:105
  67.1 5.7 %copy-start.9 = (bf16[8,96,2048]{2,1,0:T(8,128)(2,1)S(1)}, bf16[8,96,2048]{2,1,0:T(8,128)(2,1)}, u32[]{:S(2)}) copy-start(bf16[8,96,2048]{2,1,0:T(8,128)(2,1)} %all-gather.5.cloned.1.call-done) | copy-start | bytes 9437188
  110.5 12.1 %all-to-all-start.4 = ((bf16[8,1,96]{2,1,0:T(2,128)(2,1)}), bf16[8,1,96]{2,1,0:T(2,128)(2,1)S(1)}, u32[]{:S(2)}, u32[]{:S(2)}) async-start(bf16[8,1,96]{2,1,0:T(2,128)(2,1)} %copy.80), calls=%async_computation.5 | async-start | bytes 8192 | tf_op jit(solution)/shard_map/all_to_all | solution.py:131
  116.2 60.2 %reduce-scatter.5.cloned.1.call-start = ((), (), s32[]{:S(2)}) async-start(), calls=%async_computation.9 | async-start | bytes 3932160 | tf_op jit(solution)/shard_map/reduce_scatter | solution.py:120
  122.8 12.7 %copy-start.8 = (f32[1,128,2,1]{1,0,3,2:T(1,128)}, f32[1,128,2,1]{1,0,3,2:T(1,128)S(1)}, u32[]{:S(2)}) copy-start(f32[1,128,2,1]{1,0,3,2:T(1,128)S(1)} %fusion.23) | copy-start | bytes 3076
  135.5 1.9 copy-start.3
  135.5 1.9 copy-start.1
  135.5 2.2 copy-start.4
  141.3 174.1 %reduce-scatter.7.cloned.1.call-start = ((), (), s32[]{:S(2)}) async-start(), calls=%async_computation.10 | async-start | bytes 1081344
  176.4 140.3 %all-to-all-start.3 = ((bf16[8,96,512]{2,1,0:T(8,128)(2,1)}), bf16[8,96,512]{2,1,0:T(8,128)(2,1)S(1)}, u32[]{:S(2)}, u32[]{:S(2)}) async-start(bf16[8,96,512]{2,1,0:T(8,128)(2,1)} %reduce-scatter.5.cloned.1.call-done), calls=%async_computation.4 | async-start | bytes 1572864 | tf_op jit(solution)/shard_map/all_to_all | solution.py:128
  181.9 5.4 %copy-start.11 = (bf16[8,96,2048]{2,1,0:T(8,128)(2,1)S(1)}, bf16[8,96,2048]{2,1,0:T(8,128)(2,1)}, u32[]{:S(2)}) copy-start(bf16[8,96,2048]{2,1,0:T(8,128)(2,1)} %all-gather.3.cloned.1.call-done) | copy-start | bytes 9437188
  181.9 5.4 %copy-start.12 = (bf16[768,512]{0,1:T(8,128)(2,1)S(1)}, bf16[768,512]{0,1:T(8,128)(2,1)}, u32[]{:S(2)}) copy-start(bf16[768,512]{0,1:T(8,128)(2,1)} %get-tuple-element.11) | copy-start | bytes 2359300
  187.3 3.3 %copy-start.2 = (bf16[768,512]{0,1:T(8,128)(2,1)S(1)}, bf16[768,512]{0,1:T(8,128)(2,1)}, u32[]{:S(2)}) copy-start(bf16[768,512]{0,1:T(8,128)(2,1)} %copy-done.1) | copy-start | bytes 2359300
  187.3 3.3 %copy-start.10 = (bf16[8,96,2048]{2,1,0:T(8,128)(2,1)S(1)}, bf16[8,96,2048]{2,1,0:T(8,128)(2,1)}, u32[]{:S(2)}) copy-start(bf16[8,96,2048]{2,1,0:T(8,128)(2,1)} %all-gather.5.cloned.1.call-done) | copy-start | bytes 9437188
Sparse Core Ops, SparseCore 0:
  39.6 27.5 all-gather.4
  68.7 28.4 all-gather.2
  141.4 34.9 reduce-scatter.4
  178.5 136.7 reduce-scatter.6
where the time goes:
time: 326 us; the launch traced here: 325 us
  waiting for transfers between devices  185 us (57%)
  blocking collectives  65.4 us (20%)
  matrix products  39.1 us (12%)
  between operations  14.1 us (4%)
  starting transfers between devices  11.3 us (3%)
  other arithmetic  5.65 us (2%)
  local copies, waits for them, and re-layouts  4.82 us (1%)
    unnamed x5, waiting for transfers between devices  122 us
    reduce_scatter x1, waiting for transfers between devices, shards(): lax.psum_scatter(partial_dx.reshape(ep_count, capacity, width).astype(jnp...  33.2 us
    all_to_all x1, blocking collectives, shards(): lax.all_to_all(pack_rows(tok_part), 'ep', split_axis=0, concat_axis=0, ti...  27.3 us
    all_to_all x1, blocking collectives, shards(): lax.all_to_all(pack_rows(cot_part), 'ep', split_axis=0, concat_axis=0, ti...  23.3 us
    all_gather x1, waiting for transfers between devices, shards(): lax.all_gather(recv_cot_part, 'tp', axis=2, tiled=True)  21.4 us
    all_to_all x1, blocking collectives, shards(): lax.all_to_all(gate_out, 'ep', split_axis=0, concat_axis=0, tiled=True)  8.86 us
    dot_general x1, matrix products, expert_grads(): lax.dot_general(cot_in, down_weight, (((1,), (1,)), ((), ())), preferred_...  6.74 us
  transfers between devices with their start and end apart: 6, of which 5 were waited for; matrix products, arithmetic and copies ran while one was open for 8% of the time, Pallas kernels for 0%

commit v1 on v0

--- a/solution.py
+++ b/solution.py
@@ -102,7 +102,7 @@
     )
     recv_rows, recv_cot = (
         lax.all_gather(recv_part, "tp", axis=2, tiled=True),
-        lax.all_gather(recv_cot_part, "tp", axis=2, tiled=True),
+        jnp.concatenate(lax.all_gather(recv_cot_part, "tp"), axis=2),
     )
     rows_in = recv_rows.reshape(-1, width)
     cot_in = recv_cot.reshape(-1, width)

time: 326 us -> 331 us (1.015)
  local copies, waits for them, and re-layouts: 4.82 us -> 12.8 us
  matrix products: 39.1 us -> 35.6 us
    reshape x0 -> x1, local copies, waits for them, and re-layouts: none -> 4.32 us  [shards(): jnp.concatenate(lax.all_gather(recv_cot_part, 'tp'), axis=2)]
    unnamed x29 -> x38, local copies, waits for them, and re-layouts: 2.68 us -> 6.33 us
    dot_general x1, matrix products: 6.74 us -> 3.35 us  [expert_grads(): lax.dot_general(cot_in, down_weight, (((1,), (1,)), ((), ())), preferred_...]
where the time goes in v1:
time: 331 us; the launch traced here: 330 us
  waiting for transfers between devices  185 us (56%)
  blocking collectives  65.5 us (20%)
  matrix products  35.6 us (11%)
  between operations  14.1 us (4%)
  local copies, waits for them, and re-layouts  12.8 us (4%)
  starting transfers between devices  11.3 us (3%)
  other arithmetic  5.65 us (2%)
    unnamed x5, waiting for transfers between devices  122 us
    reduce_scatter x1, waiting for transfers between devices, shards(): lax.psum_scatter(partial_dx.reshape(ep_count, capacity, width).astype(jnp...  33.2 us
    all_to_all x1, blocking collectives, shards(): lax.all_to_all(pack_rows(tok_part), 'ep', split_axis=0, concat_axis=0, ti...  27.3 us
    all_to_all x1, blocking collectives, shards(): lax.all_to_all(pack_rows(cot_part), 'ep', split_axis=0, concat_axis=0, ti...  23.3 us
    all_gather x1, waiting for transfers between devices, shards(): lax.all_gather(recv_cot_part, 'tp')  21.4 us
    all_to_all x1, blocking collectives, shards(): lax.all_to_all(gate_out, 'ep', split_axis=0, concat_axis=0, tiled=True)  9.04 us
  transfers between devices with their start and end apart: 6, of which 5 were waited for; matrix products, arithmetic and copies ran while one was open for 8% of the time, Pallas kernels for 0%

profile of v1, /device:TPU:0, one launch (start us, length us, event | category | flops | bytes accessed | tf_op | source)
XLA Modules:
  0.0 330.0 jit_solution(1605193063481447364)
XLA Ops:
  7.2 0.9 copy.86
  8.3 1.2 reduce-window.6
  9.8 0.7 fusion.37
  10.9 1.2 convolution_convert_fusion.2
  12.1 27.3 %all_to_all.33 = bf16[8,96,512]{2,1,0:T(8,128)(2,1)} all-to-all(bf16[8,96,512]{2,1,0:T(8,128)(2,1)S(1)} %bitcast.89), channel_id=1, replica_groups=mesh['ep'=8,'tp'=4] {'ep'}, dimensions={0} | all-to-all | bytes 1572864 | tf_op jit(solution)/shard_map/all_to_all | solution.py:99
  39.5 1.2 convolution_convert_fusion.3
  40.8 23.3 %all_to_all.34 = bf16[8,96,512]{2,1,0:T(8,128)(2,1)} all-to-all(bf16[8,96,512]{2,1,0:T(8,128)(2,1)S(1)} %bitcast.90), channel_id=1, replica_groups=mesh['ep'=8,'tp'=4] {'ep'}, dimensions={0} | all-to-all | bytes 1572864 | tf_op jit(solution)/shard_map/all_to_all | solution.py:100
  64.7 2.4 all-gather.4.cloned.1.call-done
  67.1 5.7 %fusion.11 = f32[768,512]{0,1:T(8,128)} fusion(bf16[768,2048]{1,0:T(8,128)(2,1)} %bitcast.104, bf16[1,2048,512]{2,1,0:T(8,128)(2,1)} %param.12), kind=kOutput, calls=%fused_computation.15 | convolution fusion | flops 1610612736 | bytes 6815744 | tf_op jit(solution)/shard_map/dot_general | solution.py:37
  72.8 3.0 fusion.8
  75.8 21.4 %all-gather.6.cloned.1.call-done = bf16[32,96,512]{2,1,0:T(8,128)(2,1)} async-done(((bf16[8,96,512]{2,1,0:T(8,128)(2,1)}), bf16[32,96,512]{2,1,0:T(8,128)(2,1)}) %all-gather.6.cloned.1.call-update) | async-done | bytes 3145744 | tf_op jit(solution)/shard_map/all_gather | solution.py:105
  97.2 4.3 %copy.94 = bf16[8,96,4,512]{3,2,1,0:T(4,128)(2,1)S(1)} copy(bf16[8,96,4,512]{3,1,0,2:T(8,128)(2,1)} %bitcast.88) | data formatting | bytes 6291456 | tf_op jit(solution)/shard_map/reshape | solution.py:105
  101.6 1.0 copy.104
  103.4 1.8 copy-done.15
  105.3 3.3 %multiply_reduce_fusion = (f32[768]{0:T(1024)S(1)}, bf16[768,512]{0,1:T(8,128)(2,1)}, f32[768,512]{0,1:T(8,128)}) fusion(f32[768,512]{0,1:T(8,128)S(1)} %copy-done.7, f32[768,512]{0,1:T(8,128)S(1)} %copy-done.8, bf16[768,2048]{1,0:T(8,128)(2,1)S(1)} %bitcast.86, bf16[1,512,2048]{2,1,0:T(8,128)(2,1)S(1)} %copy-done.15), kind=kOutput, calls=%fused_computation.20 | convolution fusion | flops 1614150912 | bytes 10750976 | tf_op jit(solution)/shard_map/dot_general | solution.py:38
  108.7 5.9 %psum.7 = bf16[8,96]{1,0:T(8,128)(2,1)S(1)} all-reduce(f32[8,96]{1,0:T(8,128)S(1)} %reshape.150), channel_id=1, replica_groups=mesh['ep'=8,'tp'=4] {'tp'}, use_global_device_ids=true, to_apply=%region_7.8 | all-reduce | flops 768 | bytes 4608 | tf_op jit(solution)/shard_map/psum | solution.py:126
  115.1 5.7 %all-to-all-start.4 = ((bf16[8,1,96]{2,1,0:T(2,128)(2,1)}), bf16[8,1,96]{2,1,0:T(2,128)(2,1)S(1)}, u32[]{:S(2)}, u32[]{:S(2)}) async-start(bf16[8,1,96]{2,1,0:T(2,128)(2,1)} %copy.97), calls=%async_computation.5 | async-start | bytes 8192 | tf_op jit(solution)/shard_map/all_to_all | solution.py:131
  121.1 6.1 %all-to-all-done.4 = bf16[8,1,96]{2,1,0:T(2,128)(2,1)S(1)} async-done(((bf16[8,1,96]{2,1,0:T(2,128)(2,1)}), bf16[8,1,96]{2,1,0:T(2,128)(2,1)S(1)}, u32[]{:S(2)}, u32[]{:S(2)}) %all-to-all-start.4) | async-done | bytes 1568 | tf_op jit(solution)/shard_map/all_to_all | solution.py:131
  128.0 9.0 %all_to_all.35 = bf16[8,1,96]{2,1,0:T(2,128)(2,1)S(1)} all-to-all(bf16[8,1,96]{2,1,0:T(2,128)(2,1)S(1)} %copy.93), channel_id=1, replica_groups=mesh['ep'=8,'tp'=4] {'ep'}, dimensions={0} | all-to-all | bytes 3072 | tf_op jit(solution)/shard_map/all_to_all | solution.py:101
  137.2 3.1 multiply_convert_fusion.7
  140.4 1.8 fusion.6
  142.5 3.5 %add_convert_fusion = bf16[768,2048]{1,0:T(8,128)(2,1)} fusion(f32[768,2048]{1,0:T(8,128)S(1)} %fusion.6, bf16[768,512]{0,1:T(8,128)(2,1)S(1)} %get-tuple-element.12, bf16[1,2048,512]{2,1,0:T(8,128)(2,1)S(1)} %copy-done.6), kind=kOutput, calls=%fused_computation.1 | convolution fusion | flops 1613758464 | bytes 12320768 | tf_op jit(solution)/shard_map/dot_general | solution.py:117
  146.2 1.8 fusion.31
  147.9 33.2 %reduce-scatter.5.cloned.1.call-done = bf16[8,96,512]{2,1,0:T(8,128)(2,1)} async-done(((bf16[8,96,2048]{2,1,0:T(8,128)(2,1)}), bf16[8,96,512]{2,1,0:T(8,128)(2,1)}) %reduce-scatter.5.cloned.1.call-update) | async-done | bytes 786448 | tf_op jit(solution)/shard_map/reduce_scatter | solution.py:120
  181.2 5.5 %all-to-all-start.3 = ((bf16[8,96,512]{2,1,0:T(8,128)(2,1)}), bf16[8,96,512]{2,1,0:T(8,128)(2,1)S(1)}, u32[]{:S(2)}, u32[]{:S(2)}) async-start(bf16[8,96,512]{2,1,0:T(8,128)(2,1)} %reduce-scatter.5.cloned.1.call-done), calls=%async_computation.4 | async-start | bytes 1572864 | tf_op jit(solution)/shard_map/all_to_all | solution.py:128
  186.7 5.4 %fusion.3 = bf16[1,2048,512]{2,1,0:T(8,128)(2,1)} fusion(bf16[768,2048]{1,0:T(8,128)(2,1)} %bitcast.105, bf16[768,512]{0,1:T(8,128)(2,1)} %copy-done.5), kind=kOutput, calls=%fused_computation.7 | convolution fusion | flops 1611661312 | bytes 6029312 | tf_op jit(solution)/shard_map/dot_general | solution.py:53
  192.1 3.2 fusion.5
  195.4 3.2 fusion.4
  198.6 121.6 %reduce-scatter.7.cloned.1.call-done = f32[64,4]{1,0:T(8,128)} async-done(((f32[2048,4]{1,0:T(8,128)}), f32[64,4]{1,0:T(8,128)}) %reduce-scatter.7.cloned.1.call-update) | async-done | bytes 1040
  320.2 1.4 copy.102
  321.8 0.7 convolution_bitcast_fusion
  322.4 1.0 fusion.16
  (83 shorter events, 4.7 us)
Async XLA Ops:
  7.2 65.6 %copy-start = (bf16[1,2048,512]{2,1,0:T(8,128)(2,1)S(1)}, bf16[1,2048,512]{2,1,0:T(8,128)(2,1)}, u32[]{:S(2)}) copy-start(bf16[1,2048,512]{2,1,0:T(8,128)(2,1)} %param.11) | copy-start | bytes 6291460
  7.2 60.0 %all-gather.4.cloned.1.call-start = ((), (), s32[]{:S(2)}) async-start(), calls=%async_computation.7 | async-start | bytes 3932160 | tf_op jit(solution)/shard_map/all_gather | solution.py:104
  39.4 24.9 %copy-start.11 = (s32[128,2]{0,1:T(2,128)S(1)}, s32[128,2]{0,1:T(2,128)}, u32[]{:S(2)}) copy-start(s32[128,2]{0,1:T(2,128)} %param.9) | copy-start | bytes 3076
  39.5 25.0 %copy-start.9 = (bf16[128,2048]{1,0:T(8,128)(2,1)S(1)}, bf16[128,2048]{1,0:T(8,128)(2,1)}, u32[]{:S(2)}) copy-start(bf16[128,2048]{1,0:T(8,128)(2,1)} %param.7) | copy-start | bytes 1572868
  39.5 25.0 %copy-start.10 = (bf16[2048,4]{0,1:T(4,128)(2,1)S(1)}, bf16[2048,4]{0,1:T(4,128)(2,1)}, u32[]{:S(2)}) copy-start(bf16[2048,4]{0,1:T(4,128)(2,1)} %param.10) | copy-start | bytes 49156
  39.5 57.8 %all-gather.6.cloned.1.call-start = ((), (), s32[]{:S(2)}) async-start(), calls=%async_computation.9 | async-start | bytes 3932160 | tf_op jit(solution)/shard_map/all_gather | solution.py:105
  67.1 5.7 %copy-start.13 = (bf16[8,96,2048]{2,1,0:T(8,128)(2,1)S(1)}, bf16[8,96,2048]{2,1,0:T(8,128)(2,1)}, u32[]{:S(2)}) copy-start(bf16[8,96,2048]{2,1,0:T(8,128)(2,1)} %all-gather.4.cloned.1.call-done) | copy-start | bytes 9437188
  101.6 1.4 copy-start.7
  101.6 1.9 copy-start.8
  101.6 3.7 %copy-start.15 = (bf16[1,512,2048]{2,1,0:T(8,128)(2,1)S(1)}, bf16[1,512,2048]{2,1,0:T(8,128)(2,1)}, u32[]{:S(2)}) copy-start(bf16[1,512,2048]{2,1,0:T(8,128)(2,1)} %param.13) | copy-start | bytes 6291460
  102.6 6.0 %copy-start.1 = (bf16[96,8,4,512]{3,1,2,0:T(8,128)(2,1)}, bf16[96,8,4,512]{3,1,2,0:T(8,128)(2,1)S(1)}, u32[]{:S(2)}) copy-start(bf16[96,8,4,512]{3,1,2,0:T(8,128)(2,1)S(1)} %copy.104) | copy-start | bytes 9437188
  115.1 12.1 %all-to-all-start.4 = ((bf16[8,1,96]{2,1,0:T(2,128)(2,1)}), bf16[8,1,96]{2,1,0:T(2,128)(2,1)S(1)}, u32[]{:S(2)}, u32[]{:S(2)}) async-start(bf16[8,1,96]{2,1,0:T(2,128)(2,1)} %copy.97), calls=%async_computation.5 | async-start | bytes 8192 | tf_op jit(solution)/shard_map/all_to_all | solution.py:131
  120.8 60.4 %reduce-scatter.5.cloned.1.call-start = ((), (), s32[]{:S(2)}) async-start(), calls=%async_computation.8 | async-start | bytes 3932160 | tf_op jit(solution)/shard_map/reduce_scatter | solution.py:120
  127.4 12.9 %copy-start.12 = (f32[1,128,2,1]{1,0,3,2:T(1,128)}, f32[1,128,2,1]{1,0,3,2:T(1,128)S(1)}, u32[]{:S(2)}) copy-start(f32[1,128,2,1]{1,0,3,2:T(1,128)S(1)} %fusion.23) | copy-start | bytes 3076
  140.3 1.9 copy-start.5
  140.3 1.9 copy-start.3
  140.3 2.2 copy-start.6
  146.1 174.1 %reduce-scatter.7.cloned.1.call-start = ((), (), s32[]{:S(2)}) async-start(), calls=%async_computation.10 | async-start | bytes 1081344
  181.2 140.4 %all-to-all-start.3 = ((bf16[8,96,512]{2,1,0:T(8,128)(2,1)}), bf16[8,96,512]{2,1,0:T(8,128)(2,1)S(1)}, u32[]{:S(2)}, u32[]{:S(2)}) async-start(bf16[8,96,512]{2,1,0:T(8,128)(2,1)} %reduce-scatter.5.cloned.1.call-done), calls=%async_computation.4 | async-start | bytes 1572864 | tf_op jit(solution)/shard_map/all_to_all | solution.py:128
  186.7 5.4 %copy-start.2 = (bf16[96,8,4,512]{3,1,2,0:T(8,128)(2,1)S(1)}, bf16[96,8,4,512]{3,1,2,0:T(8,128)(2,1)}, u32[]{:S(2)}) copy-start(bf16[96,8,4,512]{3,1,2,0:T(8,128)(2,1)} %copy-done.1) | copy-start | bytes 9437188
  186.7 5.4 %copy-start.16 = (bf16[768,512]{0,1:T(8,128)(2,1)S(1)}, bf16[768,512]{0,1:T(8,128)(2,1)}, u32[]{:S(2)}) copy-start(bf16[768,512]{0,1:T(8,128)(2,1)} %get-tuple-element.11) | copy-start | bytes 2359300
  192.1 3.3 copy-start.4
  192.1 3.3 copy-start.14
Sparse Core Ops, SparseCore 0:
  39.6 27.5 all-gather.3
  68.7 28.4 all-gather.5
  146.2 34.9 reduce-scatter.4
  183.3 136.8 reduce-scatter.6
